TPU v7x, 32 devices: a whole 2x2x4 slice. The times are simulated.
32 devices in a mesh: grp: 2 (over y), sp: 4 (over z), tp: 4 (over x, core).
Axes of the slice: x: 2, y: 2, z: 4, core: 2. Of those that a mesh axis runs over, the one named last changes fastest.
Arguments:
- tokens: bfloat16 [4096, 2048], P(('grp', 'sp', 'tp')), parts along dimension 0, may hold values from -6 to 6
- norm_gain: bfloat16 [2048], replicated, may hold values from 0.099609375 to 1.8984375
- conv_outer_weight: bfloat16 [2048, 1024], P('sp', 'tp'), may hold values from -0.125 to 0.125
- conv_inner_weight: bfloat16 [2048, 1024], P('sp', 'tp'), may hold values from -0.125 to 0.125
- conv_input_weight: bfloat16 [2048, 1024], P('sp', 'tp'), may hold values from -0.125 to 0.125
- query_matrix: bfloat16 [2048, 1024], P('sp', 'tp'), may hold values from -0.125 to 0.125
- key_weight: bfloat16 [2048, 1024], P('sp', 'tp'), may hold values from -0.125 to 0.125
- value_weight: bfloat16 [2048, 1024], P('sp', 'tp'), may hold values from -0.125 to 0.125
- gate_weight: bfloat16 [2048, 1024], P('sp', 'tp'), may hold values from -0.125 to 0.125
- conv_taps: bfloat16 [3, 1024], P(None, 'tp'), may hold values from -3.5 to 3.5
- conv_out_weight: bfloat16 [1024, 2048], P('tp', 'sp'), may hold values from -0.125 to 0.125
- ret_out_weight: bfloat16 [1024, 2048], P('tp', 'sp'), may hold values from -0.125 to 0.125
- log_decay: float32 [4096, 8], P(('grp', 'sp'), 'tp'), parts along dimension 0, may hold values from -0.75 to 0
Outputs:
- mixed: bfloat16 [4096, 2048], P(('grp', 'sp', 'tp')), parts along dimension 0
There are 2 independent parts, one for each index of `grp`. A program takes and returns all parts, laid end to end along the dimension named above; an argument that names none is the same for every part. Nothing has to cross between parts.
All inputs are finite; a program needn't handle non-finite values.
Results may differ from a plain program's by a relative error of at most 0.025.
Values may be sent and summed in bfloat16 or wider, within the bound.
A program may use at most 64 MiB of HBM per device.

v0:
```python
import jax
import jax.numpy as jnp
from jax import lax
from jax.sharding import PartitionSpec as P

HEAD = 128
CONV_K = 3
BLOCK = 128
EPSILON = 1e-06
ROTARY_BASE = 10000.0
HIGHEST_PRECISION = lax.Precision.HIGHEST


def prefix_2(x, axis, join, neutral):
    place = lax.axis_index(axis)
    gathered = jax.tree.map(
        lambda a, kind: lax.all_gather(a.astype(kind), axis), x, (jnp.bfloat16, jnp.bfloat16)
    )
    state = jax.tree.map(lambda a, e: jnp.zeros_like(a) + jnp.asarray(e, a.dtype), x, neutral)

    def one(turn, state):
        return join(
            state,
            jax.tree.map(
                lambda a, own: lax.dynamic_index_in_dim(a, turn, 0, False).astype(own.dtype),
                gathered,
                x,
            ),
        )

    return lax.fori_loop(0, place, one, state)


def shifted(x, axis, by):
    count = lax.axis_size(axis)
    pairs = [(i, i + by) for i in range(count) if 0 <= i + by < count]
    return lax.ppermute(x, axis, pairs)


def rotate(head_data, positions):
    half_width = head_data.shape[-1] // 2
    inv_freq = ROTARY_BASE ** (-jnp.arange(half_width, dtype=jnp.float32) / half_width)
    angles = positions[:, None] * inv_freq[None, :]
    cosine = jnp.cos(angles)[:, None, :]
    sine_part = jnp.sin(angles)[:, None, :]
    first_half = head_data[..., :half_width]
    second_half = head_data[..., half_width:]
    return jnp.concatenate(
        [
            first_half * cosine - second_half * sine_part,
            second_half * cosine + first_half * sine_part,
        ],
        axis=-1,
    )


def head_norm(head_data):
    return head_data * lax.rsqrt(jnp.mean(head_data * head_data, axis=-1, keepdims=True) + EPSILON)


def combine_states(earlier, later):
    return (earlier[0] * later[0], later[0][:, None, None] * earlier[1] + later[1])


def body(
    tokens,
    norm_gain,
    conv_outer_weight,
    conv_inner_weight,
    conv_input_weight,
    query_matrix,
    key_weight,
    value_weight,
    gate_weight,
    conv_taps,
    conv_out_weight,
    ret_out_weight,
    log_decay,
):
    values32 = tokens.astype(jnp.float32)
    normed = (
        values32
        * lax.rsqrt(jnp.mean(values32 * values32, axis=-1, keepdims=True) + EPSILON)
        * norm_gain.astype(jnp.float32)
    ).astype(jnp.bfloat16)
    gathered = lax.all_gather(normed, "tp", axis=0, tiled=True)
    row_total = gathered.shape[0]
    whole = (
        lax.all_gather(conv_outer_weight, "sp", axis=0, tiled=True),
        lax.all_gather(conv_inner_weight, "sp", axis=0, tiled=True),
        lax.all_gather(conv_input_weight, "sp", axis=0, tiled=True),
        lax.all_gather(query_matrix, "sp", axis=0, tiled=True),
        lax.all_gather(key_weight, "sp", axis=0, tiled=True),
        lax.all_gather(value_weight, "sp", axis=0, tiled=True),
        lax.all_gather(gate_weight, "sp", axis=0, tiled=True),
    )
    projected = tuple(
        (
            jnp.dot(gathered, weight, preferred_element_type=jnp.float32).astype(jnp.bfloat16)
            for weight in whole
        )
    )
    conv_outer, conv_inner, conv_input, query_proj, key_proj, value_proj, gate_proj = projected
    heads_here = query_proj.shape[1] // HEAD
    offset = (lax.axis_index("sp") * row_total).astype(jnp.float32)
    positions = offset + jnp.arange(row_total, dtype=jnp.float32)
    head_shape = (row_total, heads_here, HEAD)
    queries = rotate(query_proj.astype(jnp.float32).reshape(head_shape), positions)
    keys_rot = rotate(key_proj.astype(jnp.float32).reshape(head_shape), positions) * HEAD ** (-0.5)
    head_values = value_proj.astype(jnp.float32).reshape(head_shape)
    block_count = row_total // BLOCK
    block_shape = (block_count, BLOCK, heads_here, HEAD)
    query_blocks = queries.reshape(block_shape)
    key_blocks = keys_rot.reshape(block_shape)
    value_blocks = head_values.reshape(block_shape)
    log_blocks = log_decay.reshape(block_count, BLOCK, heads_here)
    offsets = jnp.arange(BLOCK, dtype=jnp.int32)
    causal_mask = offsets[:, None] >= offsets[None, :]
    lower_ones = causal_mask.astype(jnp.float32)
    cumulative = jnp.einsum("ij,njh->nih", lower_ones, log_blocks, precision=HIGHEST_PRECISION)
    block_end = cumulative[:, -1, :]
    mixed_in = conv_inner.astype(jnp.float32) * conv_input.astype(jnp.float32)
    rim = shifted(mixed_in[row_total - (CONV_K - 1) :], "sp", 1)
    extended = jnp.concatenate([rim, mixed_in], axis=0)
    taps = conv_taps.astype(jnp.float32)
    conv_out = jnp.zeros(mixed_in.shape, jnp.float32)
    for tap_index in range(CONV_K):
        conv_out = conv_out + taps[tap_index][None, :] * extended[tap_index : tap_index + row_total]
    conv_branch = (conv_outer.astype(jnp.float32) * conv_out).astype(jnp.bfloat16)
    weights = jnp.exp(block_end[:, None, :] - cumulative)
    increments = jnp.einsum(
        "njh,njhd,njhe->nhde", weights, key_blocks, value_blocks, precision=HIGHEST_PRECISION
    )

    def carry_on(carried, pieces):
        block_decay, increment = pieces
        return (block_decay[:, None, None] * carried + increment, carried)

    start_state = jnp.zeros((heads_here, HEAD, HEAD), jnp.float32)
    local_end, local_before = lax.scan(carry_on, start_state, (jnp.exp(block_end), increments))
    device_decay = jnp.exp(jnp.sum(block_end, axis=0))
    incoming = prefix_2(
        (device_decay, local_end),
        "sp",
        combine_states,
        (jnp.ones_like(device_decay), jnp.zeros_like(local_end)),
    )
    local_before, incoming_state = (local_before, incoming[1])
    spread = cumulative[:, :, None, :] - cumulative[:, None, :, :]
    grid_mask = causal_mask[None, :, :, None]
    decay_grid = jnp.where(grid_mask, jnp.exp(jnp.where(grid_mask, spread, 0.0)), 0.0)
    scores = (
        jnp.einsum("nihd,njhd->nijh", query_blocks, key_blocks, precision=HIGHEST_PRECISION)
        * decay_grid
    )
    within = jnp.einsum("nijh,njhe->nihe", scores, value_blocks, precision=HIGHEST_PRECISION)
    prefix = jnp.exp(jnp.cumsum(block_end, axis=0) - block_end)
    before = local_before + prefix[:, :, None, None] * incoming_state[None]
    across = jnp.einsum("nihd,nhde->nihe", query_blocks, before, precision=HIGHEST_PRECISION)
    across = across * jnp.exp(cumulative)[..., None]
    retained = (within + across).reshape(head_shape)
    ret_branch = (
        head_norm(retained).reshape(row_total, heads_here * HEAD)
        * jax.nn.silu(gate_proj.astype(jnp.float32))
    ).astype(jnp.bfloat16)
    conv_rows_weight, ret_rows_weight = (
        lax.all_gather(conv_out_weight, "sp", axis=1, tiled=True),
        lax.all_gather(ret_out_weight, "sp", axis=1, tiled=True),
    )
    return lax.psum_scatter(
        (
            jnp.dot(conv_branch, conv_rows_weight, preferred_element_type=jnp.float32)
            + jnp.dot(ret_branch, ret_rows_weight, preferred_element_type=jnp.float32)
        ).astype(jnp.bfloat16),
        "tp",
        scatter_dimension=0,
        tiled=True,
    )


def solution(mesh):
    placed = (
        P(("grp", "sp", "tp"), None),
        P(),
        P("sp", "tp"),
        P("sp", "tp"),
        P("sp", "tp"),
        P("sp", "tp"),
        P("sp", "tp"),
        P("sp", "tp"),
        P("sp", "tp"),
        P(None, "tp"),
        P("tp", "sp"),
        P("tp", "sp"),
        P(("grp", "sp"), "tp"),
    )
    return jax.shard_map(
        body, mesh=mesh, in_specs=placed, out_specs=P(("grp", "sp", "tp"), None), check_vma=False
    )
```

profile of v0, /device:TPU:0, one launch (start us, length us, event | category | flops | bytes accessed | tf_op | source)
XLA Modules:
  0.0 343.9 jit_solution(5092971589011308150)
XLA Ops:
  6.5 0.7 all-gather.25.cloned.1.call-update
  7.3 0.7 convert_element_type.96
  8.0 1.3 fusion.9
  9.3 2.0 fusion.11
  11.4 0.7 all-gather.27.cloned.1.call-update
  13.9 0.7 all-gather.15.cloned.1.call-update
  14.6 0.7 all-gather.21.cloned.1.call-update
  15.4 0.7 all-gather.29.cloned.1.call-update
  20.9 14.0 %all-reduce = bf16[8]{0:T(256)(128)(2,1)S(1)} all-reduce(bf16[8]{0:T(256)(128)(2,1)S(1)} %dynamic-update-slice), channel_id=2, replica_groups=mesh['grp'=2,'sp'=4,'tp'=4] {'sp'}, use_global_device_ids=true, to_apply=%add | all-reduce | flops 8 | bytes 32
  37.4 1.8 multiply_cosine_fusion
  39.2 0.7 all-gather.25.cloned.1.call-done
  39.9 23.6 %all-gather.13.cloned.1.call-done = bf16[512,2048]{1,0:T(8,128)(2,1)} async-done(((bf16[128,2048]{1,0:T(8,128)(2,1)}), bf16[512,2048]{1,0:T(8,128)(2,1)}) %all-gather.13.cloned.1.call-update) | async-done | bytes 2097168 | tf_op jit(solution)/shard_map/all_gather | solution.py:86
  63.5 2.6 convolution_convert_fusion.2
  66.2 1.0 copy.95
  67.2 1.0 copy.96
  68.2 24.9 %all-gather.27.cloned.1.call-done = bf16[2048,256]{1,0:T(8,128)(2,1)} async-done(((bf16[512,256]{1,0:T(8,128)(2,1)}), bf16[2048,256]{1,0:T(8,128)(2,1)}) %all-gather.27.cloned.1.call-update) | async-done | bytes 1048592 | tf_op jit(solution)/shard_map/all_gather | solution.py:92
  93.1 2.0 convolution_convert_fusion.1
  95.1 1.0 copy.97
  96.1 1.0 copy.98
  97.1 24.8 %all-gather.23.cloned.1.call-done = bf16[2048,256]{1,0:T(8,128)(2,1)} async-done(((bf16[512,256]{1,0:T(8,128)(2,1)}), bf16[2048,256]{1,0:T(8,128)(2,1)}) %all-gather.23.cloned.1.call-update) | async-done | bytes 1048592 | tf_op jit(solution)/shard_map/all_gather | solution.py:94
  121.9 1.9 convolution_convert_fusion.3
  123.9 2.9 multiply_subtract_fusion
  126.8 1.7 fusion.23
  128.5 9.4 %while.26 = (s32[]{:T(128)}, f32[2,128,128]{2,1,0:T(8,128)S(1)}, f32[4,2,128,128]{3,2,1,0:T(8,128)}, f32[4,2]{1,0:T(4,128)}, f32[4,2,128,128]{3,2,1,0:T(8,128)}, /*index=5*/s32[]{:T(128)}, s32[]{:T(128)}) while((s32[]{:T(128)}, f32[2,128,128]{2,1,0:T(8,128)S(1)}, f32[4,2,128,128]{3,2,1,0:T(8,128)}, f32[4,2]{1,0:T(4,128)}, ...), condition=%wide.region_2.3_spmd.clone, body=%wide.region_1.2_spmd.clone.sunk | while | flops 131075 | bytes 655992 | solution.py:140
  129.1 0.7 fusion.69
  129.8 1.0 bitcast_add_fusion.2
  131.5 0.7 fusion.69
  132.1 1.0 bitcast_add_fusion.2
  133.1 0.7 bitcast_dynamic-update-slice_fusion.2
  133.8 0.7 fusion.69
  134.5 1.0 bitcast_add_fusion.2
  135.5 0.7 bitcast_dynamic-update-slice_fusion.2
  136.8 1.0 bitcast_add_fusion.2
  137.9 17.1 %all-gather.1 = bf16[8,128,128]{2,1,0:T(8,128)(2,1)} all-gather(bf16[2,128,128]{2,1,0:T(8,128)(2,1)S(1)} %convert_element_type.112), channel_id=3, replica_groups=mesh['grp'=2,'sp'=4,'tp'=4] {'sp'}, dimensions={0}, use_global_device_ids=true | all-gather | bytes 327680 | tf_op jit(solution)/shard_map/all_gather | solution.py:17
  155.0 2.7 fusion.7
  157.7 26.0 %all-gather.17.cloned.1.call-done = bf16[2048,256]{1,0:T(8,128)(2,1)} async-done(((bf16[512,256]{1,0:T(8,128)(2,1)}), bf16[2048,256]{1,0:T(8,128)(2,1)}) %all-gather.17.cloned.1.call-update) | async-done | bytes 1048592 | tf_op jit(solution)/shard_map/all_gather | solution.py:90
  183.7 2.2 fusion.6
  186.6 3.9 %collective-permute-start = (f32[2,256]{1,0:T(2,128)}, f32[2,256]{1,0:T(2,128)}, u32[]{:S(2)}, u32[]{:S(2)}) collective-permute-start(f32[2,256]{1,0:T(2,128)} %slice.45), channel_id=1, source_target_pairs={{0,4},{4,8},{8,12},{1,5},{5,9},{9,13},{2,6},{6,10},{10,14},{3,7},{... | collective-permute-start | bytes 6152 | tf_op jit(solution)/shard_map/ppermute | solution.py:37
  190.7 1.3 fusion.3
  192.5 1.9 multiply_reduce_fusion
  194.5 1.3 copy.85
  195.8 16.9 %all-gather.15.cloned.1.call-done = bf16[2048,256]{1,0:T(8,128)(2,1)} async-done(((bf16[512,256]{1,0:T(8,128)(2,1)}), bf16[2048,256]{1,0:T(8,128)(2,1)}) %all-gather.15.cloned.1.call-update) | async-done | bytes 1048592 | tf_op jit(solution)/shard_map/all_gather | solution.py:89
  212.7 29.0 %all-gather.21.cloned.1.call-done = bf16[256,2048]{1,0:T(8,128)(2,1)} async-done(((bf16[256,512]{1,0:T(8,128)(2,1)}), bf16[256,2048]{1,0:T(8,128)(2,1)}) %all-gather.21.cloned.1.call-update) | async-done | bytes 1048592 | tf_op jit(solution)/shard_map/all_gather | solution.py:167
  241.7 5.8 %fusion.30 = f32[512,2048]{1,0:T(8,128)} fusion(bf16[256,2048]{1,0:T(8,128)(2,1)} %all-gather.21.cloned.1.call-done, f32[2,256]{1,0:T(2,128)} %collective-permute-done, f32[512,256]{1,0:T(8,128)S(1)} %copy-done.2, bf16[512,2048]{1,0:T(8,128)(2,1)S(1)} %copy-done, bf16[2048,256]{1,0:T(8,128)(2,1)} %all-gather.15.cloned.1.call-done, f32[256]{0:T(256)S(1)} %bitcast.101, ...), kind=kOutput, calls=%fused_computation.62 | convolution fusion | flops 1075183616 | bytes 8918016 | tf_op jit(solution)/shard_map/dot_general | solution.py:172
  247.5 23.1 %all-gather.29.cloned.1.call-done = bf16[2048,256]{1,0:T(8,128)(2,1)} async-done(((bf16[512,256]{1,0:T(8,128)(2,1)}), bf16[2048,256]{1,0:T(8,128)(2,1)}) %all-gather.29.cloned.1.call-update) | async-done | bytes 1048592 | tf_op jit(solution)/shard_map/all_gather | solution.py:95
  270.6 28.8 %all-gather.31.cloned.1.call-done = bf16[256,2048]{1,0:T(8,128)(2,1)} async-done(((bf16[256,512]{1,0:T(8,128)(2,1)}), bf16[256,2048]{1,0:T(8,128)(2,1)}) %all-gather.31.cloned.1.call-update) | async-done | bytes 1048592 | tf_op jit(solution)/shard_map/all_gather | solution.py:168
  300.0 6.5 %add_convert_fusion = bf16[512,2048]{1,0:T(8,128)(2,1)} fusion(f32[512,2048]{1,0:T(8,128)} %fusion.30, bf16[256,2048]{1,0:T(8,128)(2,1)} %all-gather.31.cloned.1.call-done, f32[64,8,2,128]{3,2,1,0:T(2,128)S(1)} %bitcast.95, f32[64,8,2,128]{3,2,1,0:T(2,128)S(1)} %bitcast.94, bf16[512,2048]{1,0:T(8,128)(2,1)S(1)} %copy-done, ...), kind=kOutput, calls=%fused_computation.6 | convolution fusion | flops 1077018624 | bytes 11534336 | tf_op jit(solution)/shard_map/dot_general | solution.py:173
  306.6 30.7 %reduce-scatter.2.cloned.1.call-done = bf16[128,2048]{1,0:T(8,128)(2,1)} async-done(((bf16[512,2048]{1,0:T(8,128)(2,1)}), bf16[128,2048]{1,0:T(8,128)(2,1)}) %reduce-scatter.2.cloned.1.call-update) | async-done | bytes 524304 | tf_op jit(solution)/shard_map/reduce_scatter | solution.py:170
  (90 shorter events, 12.9 us)
Async XLA Ops:
  6.5 33.4 %all-gather.25.cloned.1.call-start = ((), (), s32[]{:S(2)}) async-start(), calls=%async_computation.7 | async-start | bytes 1310720 | tf_op jit(solution)/shard_map/all_gather | solution.py:93
  7.3 56.2 %all-gather.13.cloned.1.call-start = ((), (), s32[]{:S(2)}) async-start(), calls=%async_computation.1 | async-start | bytes 2621440 | tf_op jit(solution)/shard_map/all_gather | solution.py:86
  8.0 8.7 %copy-start.14 = (f32[512,2]{0,1:T(2,128)S(1)}, f32[512,2]{0,1:T(2,128)}, u32[]{:S(2)}) copy-start(f32[512,2]{0,1:T(2,128)} %param.29) | copy-start | bytes 12292
  8.0 10.7 %copy-start.15 = (u32[32]{0:T(128)S(1)}, u32[32]{0:T(128)}, u32[]{:S(2)}) copy-start(u32[32]{0:T(128)} %constant.65) | copy-start | bytes 388
  8.0 28.8 %copy-start.10 = (bf16[3,256]{1,0:T(4,128)(2,1)S(1)}, bf16[3,256]{1,0:T(4,128)(2,1)}, u32[]{:S(2)}) copy-start(bf16[3,256]{1,0:T(4,128)(2,1)} %param.26) | copy-start | bytes 4612
  11.3 81.8 %all-gather.27.cloned.1.call-start = ((), (), s32[]{:S(2)}) async-start(), calls=%async_computation.8 | async-start | bytes 1310720 | tf_op jit(solution)/shard_map/all_gather | solution.py:92
  12.1 109.8 %all-gather.23.cloned.1.call-start = ((), (), s32[]{:S(2)}) async-start(), calls=%async_computation.6 | async-start | bytes 1310720 | tf_op jit(solution)/shard_map/all_gather | solution.py:94
  12.6 142.4 %all-gather.19.cloned.1.call-start = ((), (), s32[]{:S(2)}) async-start(), calls=%async_computation.4 | async-start | bytes 1310720 | tf_op jit(solution)/shard_map/all_gather | solution.py:91
  13.2 170.5 %all-gather.17.cloned.1.call-start = ((), (), s32[]{:S(2)}) async-start(), calls=%async_computation.3 | async-start | bytes 1310720 | tf_op jit(solution)/shard_map/all_gather | solution.py:90
  13.8 198.9 %all-gather.15.cloned.1.call-start = ((), (), s32[]{:S(2)}) async-start(), calls=%async_computation.2 | async-start | bytes 1310720 | tf_op jit(solution)/shard_map/all_gather | solution.py:89
  14.6 227.1 %all-gather.21.cloned.1.call-start = ((), (), s32[]{:S(2)}) async-start(), calls=%async_computation.5 | async-start | bytes 1310720 | tf_op jit(solution)/shard_map/all_gather | solution.py:167
  15.3 255.3 %all-gather.29.cloned.1.call-start = ((), (), s32[]{:S(2)}) async-start(), calls=%async_computation.9 | async-start | bytes 1310720 | tf_op jit(solution)/shard_map/all_gather | solution.py:95
  16.0 283.4 %all-gather.31.cloned.1.call-start = ((), (), s32[]{:S(2)}) async-start(), calls=%async_computation.10 | async-start | bytes 1310720 | tf_op jit(solution)/shard_map/all_gather | solution.py:168
  16.6 320.7 %reduce-scatter.2.cloned.1.call-start = ((), (), s32[]{:S(2)}) async-start(), calls=%async_computation.11 | async-start | bytes 2621440 | tf_op jit(solution)/shard_map/reduce_scatter | solution.py:170
  66.1 27.0 %copy-start = (bf16[512,2048]{1,0:T(8,128)(2,1)S(1)}, bf16[512,2048]{1,0:T(8,128)(2,1)}, u32[]{:S(2)}) copy-start(bf16[512,2048]{1,0:T(8,128)(2,1)} %all-gather.13.cloned.1.call-done) | copy-start | bytes 6291460
  123.9 2.9 copy-start.8
  183.7 6.7 %copy-start.3 = (f32[512,2,64]{2,0,1:T(8,128)S(1)}, f32[512,2,64]{2,0,1:T(8,128)}, u32[]{:S(2)}) copy-start(f32[512,2,64]{2,0,1:T(8,128)} %get-tuple-element.140) | copy-start | bytes 786436
  183.7 6.7 %copy-start.4 = (f32[512,2,64]{2,0,1:T(8,128)S(1)}, f32[512,2,64]{2,0,1:T(8,128)}, u32[]{:S(2)}) copy-start(f32[512,2,64]{2,0,1:T(8,128)} %get-tuple-element.141) | copy-start | bytes 786436
  183.7 6.9 %copy-start.6 = (f32[4,128,2]{1,2,0:T(2,128)S(1)}, f32[4,128,2]{1,2,0:T(2,128)}, u32[]{:S(2)}) copy-start(f32[4,128,2]{1,2,0:T(2,128)} %copy.73) | copy-start | bytes 12292
  185.9 4.5 %copy-start.1 = (f32[512,256]{1,0:T(8,128)}, f32[512,256]{1,0:T(8,128)S(1)}, u32[]{:S(2)}) copy-start(f32[512,256]{1,0:T(8,128)S(1)} %fusion.6) | copy-start | bytes 1572868
  186.6 55.1 %collective-permute-start = (f32[2,256]{1,0:T(2,128)}, f32[2,256]{1,0:T(2,128)}, u32[]{:S(2)}, u32[]{:S(2)}) collective-permute-start(f32[2,256]{1,0:T(2,128)} %slice.45), channel_id=1, source_target_pairs={{0,4},{4,8},{8,12},{1,5},{5,9},{9,13},{2,6},{6,10},{10,14},{3,7},{... | collective-permute-start | bytes 6152 | tf_op jit(solution)/shard_map/ppermute | solution.py:37
  190.6 1.8 copy-start.5
  190.7 1.8 copy-start.7
  190.7 1.8 copy-start.9
  192.4 49.2 %copy-start.2 = (f32[512,256]{1,0:T(8,128)S(1)}, f32[512,256]{1,0:T(8,128)}, u32[]{:S(2)}) copy-start(f32[512,256]{1,0:T(8,128)} %copy-done.1) | copy-start | bytes 1572868
  192.4 49.2 %copy-start.11 = (f32[1,256]{1,0:T(1,128)S(1)}, f32[1,256]{1,0:T(1,128)}, u32[]{:S(2)}) copy-start(f32[1,256]{1,0:T(1,128)} %get-tuple-element.154) | copy-start | bytes 3076
  192.4 49.2 %copy-start.12 = (f32[1,256]{1,0:T(1,128)S(1)}, f32[1,256]{1,0:T(1,128)}, u32[]{:S(2)}) copy-start(f32[1,256]{1,0:T(1,128)} %get-tuple-element.155) | copy-start | bytes 3076
  192.4 49.2 %copy-start.13 = (f32[1,256]{1,0:T(1,128)S(1)}, f32[1,256]{1,0:T(1,128)}, u32[]{:S(2)}) copy-start(f32[1,256]{1,0:T(1,128)} %get-tuple-element.156) | copy-start | bytes 3076
Sparse Core Ops, SparseCore 0:
  8.9 30.9 all-gather.24
  41.5 21.9 all-gather.12
  65.1 27.9 all-gather.26
  94.5 27.3 all-gather.22
  123.3 31.5 all-gather.18
  156.4 27.3 all-gather.16
  185.3 27.3 all-gather.14
  214.3 27.3 all-gather.20
  243.2 27.3 all-gather.28
  272.0 27.3 all-gather.30
  306.7 30.5 reduce-scatter.1
where the time goes:
time: 345 us; the launch traced here: 344 us
  waiting for transfers between devices  234 us (68%)
  blocking collectives  31.1 us (9%)
  matrix products  29.2 us (8%)
  other arithmetic  16 us (5%)
  local copies, waits for them, and re-layouts  15 us (4%)
  between operations  14.2 us (4%)
  starting transfers between devices  4.26 us (1%)
    reduce_scatter x1, waiting for transfers between devices, body(): lax.psum_scatter((jnp.dot(conv_branch, conv_rows_weight, preferred_elemen...  30.7 us
    all_gather x1, waiting for transfers between devices, body(): lax.all_gather(conv_out_weight, 'sp', axis=1, tiled=True)  29 us
    all_gather x1, waiting for transfers between devices, body(): lax.all_gather(ret_out_weight, 'sp', axis=1, tiled=True)  28.8 us
    all_gather x1, waiting for transfers between devices, body(): lax.all_gather(conv_inner_weight, 'sp', axis=0, tiled=True)  26 us
    all_gather x1, waiting for transfers between devices, body(): lax.all_gather(query_matrix, 'sp', axis=0, tiled=True)  24.9 us
    all_gather x1, waiting for transfers between devices, body(): lax.all_gather(value_weight, 'sp', axis=0, tiled=True)  24.8 us
    all_gather x1, waiting for transfers between devices, body(): gathered = lax.all_gather(normed, 'tp', axis=0, tiled=True)  23.6 us
    all_gather x1, waiting for transfers between devices, body(): lax.all_gather(gate_weight, 'sp', axis=0, tiled=True)  23.1 us
  transfers between devices with their start and end apart: 12, of which 10 were waited for; matrix products, arithmetic and copies ran while one was open for 15% of the time, Pallas kernels for 0%

commit v1 on v0

--- a/solution.py
+++ b/solution.py
@@ -164,7 +164,7 @@
         * jax.nn.silu(gate_proj.astype(jnp.float32))
     ).astype(jnp.bfloat16)
     conv_rows_weight, ret_rows_weight = (
-        lax.all_gather(conv_out_weight, "sp", axis=1, tiled=True),
+        jnp.concatenate(lax.all_gather(conv_out_weight, "sp"), axis=1),
         lax.all_gather(ret_out_weight, "sp", axis=1, tiled=True),
     )
     return lax.psum_scatter(

time: 345 us -> 345 us (level)
    all_gather x1, waiting for transfers between devices: 29 us -> 0.74 us  [body(): lax.all_gather(conv_out_weight, 'sp')]
    all_gather x1, waiting for transfers between devices: 0.74 us -> 26.7 us  [body(): lax.all_gather(key_weight, 'sp', axis=0, tiled=True)]
  transfers between devices with their start and end apart: 12 -> 12, of which waited for: 10 -> 11; matrix products, arithmetic and copies ran while one was open for 15% -> 16% of each run, Pallas kernels for 0% -> 0%
where the time goes in v1:
time: 345 us; the launch traced here: 344 us
  waiting for transfers between devices  231 us (67%)
  blocking collectives  31.1 us (9%)
  matrix products  29.6 us (9%)
  local copies, waits for them, and re-layouts  18 us (5%)
  other arithmetic  15.9 us (5%)
  between operations  14.2 us (4%)
  starting transfers between devices  4.32 us (1%)
    reduce_scatter x1, waiting for transfers between devices, body(): lax.psum_scatter((jnp.dot(conv_branch, conv_rows_weight, preferred_elemen...  30.7 us
    all_gather x1, waiting for transfers between devices, body(): lax.all_gather(ret_out_weight, 'sp', axis=1, tiled=True)  28.8 us
    all_gather x1, waiting for transfers between devices, body(): lax.all_gather(key_weight, 'sp', axis=0, tiled=True)  26.7 us
    all_gather x1, waiting for transfers between devices, body(): lax.all_gather(conv_inner_weight, 'sp', axis=0, tiled=True)  26.1 us
    all_gather x1, waiting for transfers between devices, body(): lax.all_gather(value_weight, 'sp', axis=0, tiled=True)  24.8 us
    all_gather x1, waiting for transfers between devices, body(): lax.all_gather(query_matrix, 'sp', axis=0, tiled=True)  24.8 us
    all_gather x1, waiting for transfers between devices, body(): gathered = lax.all_gather(normed, 'tp', axis=0, tiled=True)  23.5 us
    all_gather x1, waiting for transfers between devices, body(): lax.all_gather(gate_weight, 'sp', axis=0, tiled=True)  22.8 us
  transfers between devices with their start and end apart: 12, of which 11 were waited for; matrix products, arithmetic and copies ran while one was open for 16% of the time, Pallas kernels for 0%

profile of v1, /device:TPU:0, one launch (start us, length us, event | category | flops | bytes accessed | tf_op | source)
XLA Modules:
  0.0 344.0 jit_solution(14169159024597653217)
XLA Ops:
  6.5 0.7 all-gather.32.cloned.1.call-update
  7.3 0.7 all-gather.24.cloned.1.call-update
  8.1 0.7 convert_element_type.96
  8.8 1.2 fusion.9
  10.0 2.0 fusion.11
  13.9 0.7 all-gather.18.cloned.1.call-update
  14.6 0.7 all-gather.16.cloned.1.call-update
  15.4 0.7 all-gather.28.cloned.1.call-update
  20.9 14.0 %all-reduce = bf16[8]{0:T(256)(128)(2,1)S(1)} all-reduce(bf16[8]{0:T(256)(128)(2,1)S(1)} %dynamic-update-slice), channel_id=3, replica_groups=mesh['grp'=2,'sp'=4,'tp'=4] {'sp'}, use_global_device_ids=true, to_apply=%add | all-reduce | flops 8 | bytes 32
  34.9 0.7 reshape.185
  37.4 1.8 multiply_cosine_fusion
  39.2 0.7 all-gather.32.cloned.1.call-done
  39.9 2.3 copy.88
  42.2 26.7 %all-gather.24.cloned.1.call-done = bf16[2048,256]{1,0:T(8,128)(2,1)} async-done(((bf16[512,256]{1,0:T(8,128)(2,1)}), bf16[2048,256]{1,0:T(8,128)(2,1)}) %all-gather.24.cloned.1.call-update) | async-done | bytes 1048592 | tf_op jit(solution)/shard_map/all_gather | solution.py:93
  68.9 23.5 %all-gather.14.cloned.1.call-done = bf16[512,2048]{1,0:T(8,128)(2,1)} async-done(((bf16[128,2048]{1,0:T(8,128)(2,1)}), bf16[512,2048]{1,0:T(8,128)(2,1)}) %all-gather.14.cloned.1.call-update) | async-done | bytes 2097168 | tf_op jit(solution)/shard_map/all_gather | solution.py:86
  92.4 2.6 convolution_convert_fusion.2
  95.1 1.0 copy.121
  96.1 1.0 copy.122
  97.1 24.8 %all-gather.26.cloned.1.call-done = bf16[2048,256]{1,0:T(8,128)(2,1)} async-done(((bf16[512,256]{1,0:T(8,128)(2,1)}), bf16[2048,256]{1,0:T(8,128)(2,1)}) %all-gather.26.cloned.1.call-update) | async-done | bytes 1048592 | tf_op jit(solution)/shard_map/all_gather | solution.py:92
  121.8 2.0 convolution_convert_fusion.1
  123.9 1.0 copy.123
  124.9 1.0 copy.124
  125.9 24.8 %all-gather.22.cloned.1.call-done = bf16[2048,256]{1,0:T(8,128)(2,1)} async-done(((bf16[512,256]{1,0:T(8,128)(2,1)}), bf16[2048,256]{1,0:T(8,128)(2,1)}) %all-gather.22.cloned.1.call-update) | async-done | bytes 1048592 | tf_op jit(solution)/shard_map/all_gather | solution.py:94
  150.6 1.9 convolution_convert_fusion.3
  152.7 2.9 multiply_subtract_fusion
  155.5 1.7 fusion.23
  157.2 9.3 %while.26 = (s32[]{:T(128)}, f32[2,128,128]{2,1,0:T(8,128)S(1)}, f32[4,2,128,128]{3,2,1,0:T(8,128)}, f32[4,2]{1,0:T(4,128)}, f32[4,2,128,128]{3,2,1,0:T(8,128)}, /*index=5*/s32[]{:T(128)}, s32[]{:T(128)}) while((s32[]{:T(128)}, f32[2,128,128]{2,1,0:T(8,128)S(1)}, f32[4,2,128,128]{3,2,1,0:T(8,128)}, f32[4,2]{1,0:T(4,128)}, ...), condition=%wide.region_2.3_spmd.clone, body=%wide.region_1.2_spmd.clone.sunk | while | flops 131075 | bytes 655992 | solution.py:140
  157.2 0.7 bitcast_dynamic-update-slice_fusion.2
  158.5 1.0 bitcast_add_fusion.2
  159.5 0.7 bitcast_dynamic-update-slice_fusion.2
  160.9 1.0 bitcast_add_fusion.2
  161.9 0.7 bitcast_dynamic-update-slice_fusion.2
  163.2 1.0 bitcast_add_fusion.2
  165.5 1.0 bitcast_add_fusion.2
  166.5 17.1 %all-gather.2 = bf16[8,128,128]{2,1,0:T(8,128)(2,1)} all-gather(bf16[2,128,128]{2,1,0:T(8,128)(2,1)S(1)} %convert_element_type.112), channel_id=4, replica_groups=mesh['grp'=2,'sp'=4,'tp'=4] {'sp'}, dimensions={0}, use_global_device_ids=true | all-gather | bytes 327680 | tf_op jit(solution)/shard_map/all_gather | solution.py:17
  183.8 2.7 fusion.7
  186.5 26.1 %all-gather.18.cloned.1.call-done = bf16[2048,256]{1,0:T(8,128)(2,1)} async-done(((bf16[512,256]{1,0:T(8,128)(2,1)}), bf16[2048,256]{1,0:T(8,128)(2,1)}) %all-gather.18.cloned.1.call-update) | async-done | bytes 1048592 | tf_op jit(solution)/shard_map/all_gather | solution.py:90
  212.6 2.2 fusion.6
  215.4 3.9 %collective-permute-start = (f32[2,256]{1,0:T(2,128)}, f32[2,256]{1,0:T(2,128)}, u32[]{:S(2)}, u32[]{:S(2)}) collective-permute-start(f32[2,256]{1,0:T(2,128)} %slice.45), channel_id=1, source_target_pairs={{0,4},{4,8},{8,12},{1,5},{5,9},{9,13},{2,6},{6,10},{10,14},{3,7},{... | collective-permute-start | bytes 6152 | tf_op jit(solution)/shard_map/ppermute | solution.py:37
  219.6 1.3 fusion.3
  221.4 1.9 multiply_reduce_fusion
  223.5 2.1 copy.111
  225.6 16.0 %all-gather.16.cloned.1.call-done = bf16[2048,256]{1,0:T(8,128)(2,1)} async-done(((bf16[512,256]{1,0:T(8,128)(2,1)}), bf16[2048,256]{1,0:T(8,128)(2,1)}) %all-gather.16.cloned.1.call-update) | async-done | bytes 1048592 | tf_op jit(solution)/shard_map/all_gather | solution.py:89
  241.6 6.2 %fusion.30 = f32[512,2048]{1,0:T(8,128)} fusion(bf16[256,2048]{0,1:T(8,128)(2,1)S(1)} %bitcast.98, f32[2,256]{1,0:T(2,128)} %collective-permute-done, f32[512,256]{1,0:T(8,128)} %copy-done.2, bf16[512,2048]{1,0:T(8,128)(2,1)S(1)} %copy-done, bf16[2048,256]{1,0:T(8,128)(2,1)} %all-gather.16.cloned.1.call-done, f32[256]{0:T(256)S(1)} %bitcast.107, ...), kind=kOutput, calls=%fused_computation.62 | convolution fusion | flops 1075183616 | bytes 8918016 | tf_op jit(solution)/shard_map/dot_general | solution.py:172
  247.8 22.8 %all-gather.28.cloned.1.call-done = bf16[2048,256]{1,0:T(8,128)(2,1)} async-done(((bf16[512,256]{1,0:T(8,128)(2,1)}), bf16[2048,256]{1,0:T(8,128)(2,1)}) %all-gather.28.cloned.1.call-update) | async-done | bytes 1048592 | tf_op jit(solution)/shard_map/all_gather | solution.py:95
  270.6 28.8 %all-gather.30.cloned.1.call-done = bf16[256,2048]{1,0:T(8,128)(2,1)} async-done(((bf16[256,512]{1,0:T(8,128)(2,1)}), bf16[256,2048]{1,0:T(8,128)(2,1)}) %all-gather.30.cloned.1.call-update) | async-done | bytes 1048592 | tf_op jit(solution)/shard_map/all_gather | solution.py:168
  300.0 6.7 %add_convert_fusion = bf16[512,2048]{1,0:T(8,128)(2,1)} fusion(f32[512,2048]{1,0:T(8,128)} %fusion.30, bf16[256,2048]{1,0:T(8,128)(2,1)} %all-gather.30.cloned.1.call-done, f32[64,8,2,128]{3,2,1,0:T(2,128)S(1)} %bitcast.100, f32[64,8,2,128]{3,2,1,0:T(2,128)} %bitcast.99, bf16[512,2048]{1,0:T(8,128)(2,1)S(1)} %copy-done, ...), kind=kOutput, calls=%fused_computation.6 | convolution fusion | flops 1077018624 | bytes 11534336 | tf_op jit(solution)/shard_map/dot_general | solution.py:173
  306.7 30.7 %reduce-scatter.2.cloned.1.call-done = bf16[128,2048]{1,0:T(8,128)(2,1)} async-done(((bf16[512,2048]{1,0:T(8,128)(2,1)}), bf16[128,2048]{1,0:T(8,128)(2,1)}) %reduce-scatter.2.cloned.1.call-update) | async-done | bytes 524304 | tf_op jit(solution)/shard_map/reduce_scatter | solution.py:170
  (91 shorter events, 13.6 us)
Async XLA Ops:
  6.5 33.4 %all-gather.32.cloned.1.call-start = ((), (), s32[]{:S(2)}) async-start(), calls=%async_computation.11 | async-start | bytes 1310720 | tf_op jit(solution)/shard_map/all_gather | solution.py:167
  7.3 9.5 %copy-start.14 = (f32[512,2]{0,1:T(2,128)S(1)}, f32[512,2]{0,1:T(2,128)}, u32[]{:S(2)}) copy-start(f32[512,2]{0,1:T(2,128)} %param.29) | copy-start | bytes 12292
  7.3 61.6 %all-gather.24.cloned.1.call-start = ((), (), s32[]{:S(2)}) async-start(), calls=%async_computation.6 | async-start | bytes 1310720 | tf_op jit(solution)/shard_map/all_gather | solution.py:93
  8.0 10.7 %copy-start.15 = (u32[32]{0:T(128)S(1)}, u32[32]{0:T(128)}, u32[]{:S(2)}) copy-start(u32[32]{0:T(128)} %constant.65) | copy-start | bytes 388
  8.0 28.8 %copy-start.10 = (bf16[3,256]{1,0:T(4,128)(2,1)S(1)}, bf16[3,256]{1,0:T(4,128)(2,1)}, u32[]{:S(2)}) copy-start(bf16[3,256]{1,0:T(4,128)(2,1)} %param.26) | copy-start | bytes 4612
  8.0 84.4 %all-gather.14.cloned.1.call-start = ((), (), s32[]{:S(2)}) async-start(), calls=%async_computation.1 | async-start | bytes 2621440 | tf_op jit(solution)/shard_map/all_gather | solution.py:86
  12.1 109.8 %all-gather.26.cloned.1.call-start = ((), (), s32[]{:S(2)}) async-start(), calls=%async_computation.7 | async-start | bytes 1310720 | tf_op jit(solution)/shard_map/all_gather | solution.py:92
  12.6 138.0 %all-gather.22.cloned.1.call-start = ((), (), s32[]{:S(2)}) async-start(), calls=%async_computation.5 | async-start | bytes 1310720 | tf_op jit(solution)/shard_map/all_gather | solution.py:94
  13.2 170.5 %all-gather.20.cloned.1.call-start = ((), (), s32[]{:S(2)}) async-start(), calls=%async_computation.4 | async-start | bytes 1310720 | tf_op jit(solution)/shard_map/all_gather | solution.py:91
  13.8 198.8 %all-gather.18.cloned.1.call-start = ((), (), s32[]{:S(2)}) async-start(), calls=%async_computation.3 | async-start | bytes 1310720 | tf_op jit(solution)/shard_map/all_gather | solution.py:90
  14.6 227.0 %all-gather.16.cloned.1.call-start = ((), (), s32[]{:S(2)}) async-start(), calls=%async_computation.2 | async-start | bytes 1310720 | tf_op jit(solution)/shard_map/all_gather | solution.py:89
  15.3 255.2 %all-gather.28.cloned.1.call-start = ((), (), s32[]{:S(2)}) async-start(), calls=%async_computation.8 | async-start | bytes 1310720 | tf_op jit(solution)/shard_map/all_gather | solution.py:95
  16.0 283.3 %all-gather.30.cloned.1.call-start = ((), (), s32[]{:S(2)}) async-start(), calls=%async_computation.9 | async-start | bytes 1310720 | tf_op jit(solution)/shard_map/all_gather | solution.py:168
  16.6 320.8 %reduce-scatter.2.cloned.1.call-start = ((), (), s32[]{:S(2)}) async-start(), calls=%async_computation.10 | async-start | bytes 2621440 | tf_op jit(solution)/shard_map/reduce_scatter | solution.py:170
  95.0 26.8 %copy-start = (bf16[512,2048]{1,0:T(8,128)(2,1)S(1)}, bf16[512,2048]{1,0:T(8,128)(2,1)}, u32[]{:S(2)}) copy-start(bf16[512,2048]{1,0:T(8,128)(2,1)} %all-gather.14.cloned.1.call-done) | copy-start | bytes 6291460
  152.7 2.9 copy-start.8
  212.6 6.8 %copy-start.3 = (f32[512,2,64]{2,0,1:T(8,128)S(1)}, f32[512,2,64]{2,0,1:T(8,128)}, u32[]{:S(2)}) copy-start(f32[512,2,64]{2,0,1:T(8,128)} %get-tuple-element.145) | copy-start | bytes 786436
  212.6 6.8 %copy-start.4 = (f32[512,2,64]{2,0,1:T(8,128)S(1)}, f32[512,2,64]{2,0,1:T(8,128)}, u32[]{:S(2)}) copy-start(f32[512,2,64]{2,0,1:T(8,128)} %get-tuple-element.146) | copy-start | bytes 786436
  212.6 7.0 %copy-start.6 = (f32[4,128,2]{1,2,0:T(2,128)S(1)}, f32[4,128,2]{1,2,0:T(2,128)}, u32[]{:S(2)}) copy-start(f32[4,128,2]{1,2,0:T(2,128)} %copy.99) | copy-start | bytes 12292
  214.8 4.6 %copy-start.2 = (f32[512,256]{1,0:T(8,128)}, f32[512,256]{1,0:T(8,128)S(1)}, u32[]{:S(2)}) copy-start(f32[512,256]{1,0:T(8,128)S(1)} %fusion.6) | copy-start | bytes 1572868
  215.4 26.1 %collective-permute-start = (f32[2,256]{1,0:T(2,128)}, f32[2,256]{1,0:T(2,128)}, u32[]{:S(2)}, u32[]{:S(2)}) collective-permute-start(f32[2,256]{1,0:T(2,128)} %slice.45), channel_id=1, source_target_pairs={{0,4},{4,8},{8,12},{1,5},{5,9},{9,13},{2,6},{6,10},{10,14},{3,7},{... | collective-permute-start | bytes 6152 | tf_op jit(solution)/shard_map/ppermute | solution.py:37
  219.6 1.8 copy-start.5
  219.6 1.8 copy-start.7
  219.6 1.8 copy-start.9
  221.4 20.2 %copy-start.1 = (bf16[256,4,512]{0,2,1:T(8,128)(2,1)S(1)}, bf16[256,4,512]{0,2,1:T(8,128)(2,1)}, u32[]{:S(2)}) copy-start(bf16[256,4,512]{0,2,1:T(8,128)(2,1)} %copy.88) | copy-start | bytes 3145732
  221.4 20.2 %copy-start.11 = (f32[1,256]{1,0:T(1,128)S(1)}, f32[1,256]{1,0:T(1,128)}, u32[]{:S(2)}) copy-start(f32[1,256]{1,0:T(1,128)} %get-tuple-element.159) | copy-start | bytes 3076
  221.4 20.2 %copy-start.12 = (f32[1,256]{1,0:T(1,128)S(1)}, f32[1,256]{1,0:T(1,128)}, u32[]{:S(2)}) copy-start(f32[1,256]{1,0:T(1,128)} %get-tuple-element.160) | copy-start | bytes 3076
  221.4 20.2 %copy-start.13 = (f32[1,256]{1,0:T(1,128)S(1)}, f32[1,256]{1,0:T(1,128)}, u32[]{:S(2)}) copy-start(f32[1,256]{1,0:T(1,128)} %get-tuple-element.161) | copy-start | bytes 3076
Sparse Core Ops, SparseCore 0:
  8.9 30.9 all-gather.31
  41.5 27.3 all-gather.23
  70.4 21.9 all-gather.13
  93.8 27.9 all-gather.25
  123.3 27.3 all-gather.21
  152.1 31.6 all-gather.19
  185.3 27.2 all-gather.17
  214.2 27.3 all-gather.15
  243.2 27.3 all-gather.27
  272.0 27.3 all-gather.29
  306.8 30.5 reduce-scatter.1
